TPU v7x, 512 devices: a whole 4x4x16 slice. The times are simulated.
512 devices in a mesh: ep: 32 (over z, core), tp: 16 (over y, x).
Axes of the slice: x: 4, y: 4, z: 16, core: 2. Of those that a mesh axis runs over, the one named last changes fastest.
Arguments:
- mixer_value_input: bfloat16 [8192, 4096], P('ep', 'tp'), may hold values from -6 to 6
- input_state_matrix: bfloat16 [8192, 2048], P('ep', 'tp'), may hold values from -6 to 6
- output_state_matrix: bfloat16 [8192, 2048], P('ep', 'tp'), may hold values from -6 to 6
- output_gate_input: bfloat16 [8192, 4096], P('ep', 'tp'), may hold values from -6 to 6
- step_input: float32 [8192, 64], P('ep', 'tp'), may hold values from -6 to -2
- extra_log_decay: float32 [8192, 64], P('ep', 'tp'), may hold values from -1 to 0
- head_log_decay: float32 [64], P('tp'), may hold values from -10 to 1
- head_skip_scale: float32 [64], P('tp'), may hold values from 0.5 to 2
- value_kernel: float32 [4, 4096], P(None, 'tp'), may hold values from -3 to 3
- input_matrix_kernel: float32 [4, 2048], P(None, 'tp'), may hold values from -3 to 3
- output_matrix_kernel: float32 [4, 2048], P(None, 'tp'), may hold values from -3 to 3
- mixer_norm_scale: float32 [4096], P('tp'), may hold values from 0.1 to 1.9
- mixer_output_weight: bfloat16 [4096, 2048], P(None, 'tp'), may hold values from -0.09375 to 0.09375
- second_token_rows: bfloat16 [8192, 2048], P('ep'), may hold values from -6 to 6
- expert_norm_scale: float32 [2048], replicated, may hold values from 0.1 to 1.9
- routed_expert_index: int32 [8192, 4], P('ep'), may hold values from 0 to 63, all different within a row; in each aligned block of 256 rows (0 to 255, 256 to 511, ...) at most 24 rows name the same one
- routed_expert_weight: float32 [8192, 4], P('ep'), may hold values from 0.1 to 1
- routed_gate_weight: bfloat16 [64, 2048, 1024], P('ep', None, 'tp'), may hold values from -0.125 to 0.125
- routed_up_weight: bfloat16 [64, 2048, 1024], P('ep', None, 'tp'), may hold values from -0.125 to 0.125
- routed_down_weight: bfloat16 [64, 1024, 2048], P('ep', None, 'tp'), may hold values from -0.1875 to 0.1875
- shared_gate_weight: bfloat16 [2048, 1024], P(None, 'tp'), may hold values from -0.125 to 0.125
- shared_up_weight: bfloat16 [2048, 1024], P(None, 'tp'), may hold values from -0.125 to 0.125
- shared_down_weight: bfloat16 [1024, 2048], P(None, 'tp'), may hold values from -0.1875 to 0.1875
Outputs:
- mixer_output: bfloat16 [8192, 2048], P('ep', 'tp')
- routed_out: bfloat16 [8192, 2048], P('ep', 'tp')
Inputs may be any that keep to these rules, and one draw needn't show every extreme that they name: `routed_expert_index`: in each aligned block of 256 rows (the rows of one index of ep) no expert is named more than 24 times, a bound that some block reaches.
All inputs are finite; a program needn't handle non-finite values.
Results may differ from a plain program's by a relative error of at most 0.012.
Values may be sent and summed in bfloat16 or wider, within the bound.
No kernel may reach another device: no remote copies, remote signals or barrier semaphores. Data moves between devices by JAX's collectives and lax.ppermute only.
A program may use at most 64 MiB of HBM per device.

v0:
```python
import jax
import jax.numpy as jnp
from jax import lax
from jax.sharding import PartitionSpec as P

HEAD_DIM = 64
STATE = 128
CONV_TAPS = 4
BLOCK = 128
TOP_K = 4
epsilon = 1e-05
F32 = jnp.float32
BF16 = jnp.bfloat16


def passed_along(x, axis, by):
    size = lax.axis_size(axis)
    pairs = [(i, i + by) for i in range(size) if 0 <= i + by < size]
    return lax.ppermute(x, axis, pairs)


def high(x):
    return lax.reduce_precision(x, 8, 7)


def three_parts(x):
    a = high(x)
    b = high(x - a)
    return (a, b, x - a - b)


def laid_out(tiles, dim):
    tiles = jnp.moveaxis(tiles, 0, dim)
    dims = tiles.shape
    return tiles.reshape(*dims[:dim], dims[dim] * dims[dim + 1], *dims[dim + 2 :])


def one_gather(arrays, axis, dims):
    ravelled = jnp.concatenate([a.reshape(-1) for a in arrays])
    lines, at, finished = (lax.all_gather(ravelled, axis), 0, [])
    for a, dim in zip(arrays, dims):
        tiles = lines[:, at : at + a.size].reshape(-1, *a.shape)
        finished.append(laid_out(tiles, dim))
        at += a.size
    return tuple(finished)


def conv_silu(tail_rows, source, weights):
    length = source.shape[0]
    padded = jnp.concatenate([tail_rows, source], axis=0)
    total_sum = jnp.zeros(source.shape, F32)
    for tap_index in range(CONV_TAPS):
        total_sum = (
            total_sum + padded[tap_index : tap_index + length].astype(F32) * weights[tap_index]
        )
    return jax.nn.silu(total_sum).astype(BF16)


def state_before(log_total, total_state):
    heads = log_total.shape[0]
    count = lax.axis_size("ep")
    place = lax.axis_index("ep")
    parts = jnp.stack(three_parts(log_total)).reshape(1, 3 * heads)
    row = jnp.pad(parts, ((0, 15), (0, STATE - 3 * heads)))
    rows = heads * HEAD_DIM
    payload = jnp.concatenate([total_state.reshape(rows, STATE), row], axis=0).astype(BF16)
    gathered = lax.all_gather(payload, "ep")
    tail = gathered[:, rows, : 3 * heads].astype(F32).reshape(count, 3, heads)
    logs = jnp.sum(tail, axis=1)
    at = jnp.arange(count)
    between = (at[None, :] > at[:, None]) & (at[None, :] < place)
    spans = jnp.sum(jnp.where(between[:, :, None], logs[None], 0.0), axis=1)
    weights = jnp.where((at < place)[:, None], jnp.exp(spans), 0.0)
    wide = jnp.repeat(weights, HEAD_DIM, axis=1)[:, :, None]
    summed = jnp.sum(gathered[:, :rows, :].astype(F32) * wide, axis=0)
    return summed.reshape(heads, HEAD_DIM, STATE)


def routes(index_t, weight_t, experts, capacity):
    rows = index_t.shape[1]
    ids = jnp.arange(experts, dtype=jnp.int32)[:, None]
    named = jnp.zeros((experts, rows), F32)
    weight = jnp.zeros((experts, rows), F32)
    for k in range(TOP_K):
        hit = index_t[k][None, :] == ids
        named = jnp.where(hit, 1.0, named)
        weight = jnp.where(hit, weight_t[k][None, :], weight)
    at = jnp.arange(rows)
    earlier = (at[:, None] < at[None, :]).astype(BF16)
    place = jnp.dot(named.astype(BF16), earlier, preferred_element_type=F32)
    place = jnp.where(named > 0.0, place, -1.0)
    slots = jnp.arange(capacity, dtype=jnp.int32).astype(F32)[None, :, None]
    taken = place[:, None, :] == slots
    return (taken, weight)


def on_device(
    mixer_value_input,
    input_state_matrix,
    output_state_matrix,
    output_gate_input,
    step_input,
    extra_log_decay,
    head_log_decay,
    head_skip_scale,
    value_kernel,
    input_matrix_kernel,
    output_matrix_kernel,
    mixer_norm_scale,
    mixer_output_weight,
    second_token_rows,
    expert_norm_scale,
    routed_expert_index,
    routed_expert_weight,
    routed_gate_weight,
    routed_up_weight,
    routed_down_weight,
    shared_gate_weight,
    shared_up_weight,
    shared_down_weight,
):
    length = mixer_value_input.shape[0]
    heads_local = step_input.shape[1]
    width_x = mixer_value_input.shape[1]
    width_b = input_state_matrix.shape[1]
    groups_local = width_b // STATE
    head_ratio = heads_local // groups_local
    nblocks = length // BLOCK
    lead_row = length - CONV_TAPS + 1
    edge_rows = jnp.concatenate(
        [
            mixer_value_input[lead_row:],
            input_state_matrix[lead_row:],
            output_state_matrix[lead_row:],
        ],
        axis=1,
    )
    tail_rows = passed_along(edge_rows, "ep", 1)
    values = conv_silu(tail_rows[:, :width_x], mixer_value_input, value_kernel)
    in_mat = conv_silu(
        tail_rows[:, width_x : width_x + width_b], input_state_matrix, input_matrix_kernel
    )
    out_mat = conv_silu(
        tail_rows[:, width_x + width_b :], output_state_matrix, output_matrix_kernel
    )
    step_length = jax.nn.softplus(step_input)
    decay_logarithm = -jnp.exp(head_log_decay)[None, :] * step_length + extra_log_decay
    running = jnp.cumsum(decay_logarithm.reshape(nblocks, BLOCK, heads_local), axis=1)
    value_wide = values.astype(F32).reshape(nblocks, BLOCK, heads_local, HEAD_DIM)
    scaled = value_wide * step_length.reshape(nblocks, BLOCK, heads_local)[..., None]
    in_blocks = in_mat.reshape(nblocks, BLOCK, groups_local, STATE)
    out_blocks = out_mat.reshape(nblocks, BLOCK, groups_local, STATE)
    scores = jnp.einsum("bign,bjgn->bgij", out_blocks, in_blocks, preferred_element_type=F32)
    scores = jnp.repeat(scores, head_ratio, axis=1)
    spread = jnp.transpose(running[:, :, None, :] - running[:, None, :, :], (0, 3, 1, 2))
    lower_mask = jnp.tril(jnp.ones((BLOCK, BLOCK), bool))[None, None]
    decay_mat = jnp.where(lower_mask, jnp.exp(jnp.where(lower_mask, spread, 0.0)), 0.0)
    inside = jnp.einsum("bhij,bjhp->bihp", scores * decay_mat, scaled)
    out_head = jnp.repeat(out_blocks.astype(F32), head_ratio, axis=2)
    in_head = jnp.repeat(in_blocks.astype(F32), head_ratio, axis=2)
    block_logs = running[:, -1]
    to_end = jnp.exp(block_logs[:, None, :] - running)
    block_state = jnp.einsum("bjhn,bjh,bjhp->bhpn", in_head, to_end, scaled)
    carried = jnp.zeros((heads_local, HEAD_DIM, STATE), F32)
    before = []
    for b in range(nblocks):
        before.append(carried)
        carried = carried * jnp.exp(block_logs[b])[:, None, None] + block_state[b]
    local_prev = jnp.stack(before)
    before_logs = jnp.cumsum(block_logs, axis=0) - block_logs
    incoming = state_before(jnp.sum(block_logs, axis=0), carried)
    entering = local_prev + jnp.exp(before_logs)[:, :, None, None] * incoming[None]
    carried_term = jnp.einsum("bihn,bhpn->bihp", out_head, entering) * jnp.exp(running)[..., None]
    mixed_heads = (inside + carried_term).reshape(length, heads_local, HEAD_DIM)
    mixed_heads = mixed_heads + head_skip_scale[None, :, None] * value_wide.reshape(
        length, heads_local, HEAD_DIM
    )
    gated_heads = mixed_heads * jax.nn.silu(output_gate_input.astype(F32)).reshape(
        length, heads_local, HEAD_DIM
    )
    grouped = gated_heads.reshape(length, groups_local, head_ratio * HEAD_DIM)
    grouped = grouped * lax.rsqrt(jnp.mean(grouped * grouped, axis=-1, keepdims=True) + epsilon)
    mixer_normed = (grouped.reshape(length, width_x) * mixer_norm_scale).astype(BF16)
    rows_local = second_token_rows.shape[0]
    model_width = second_token_rows.shape[1]
    local_experts = routed_gate_weight.shape[0]
    ep_count = lax.axis_size("ep")
    experts = local_experts * ep_count
    capacity = max(2, 3 * rows_local * TOP_K // (2 * experts))
    col_width = model_width // lax.axis_size("tp")
    rows_wide = second_token_rows.astype(F32)
    normed = (
        rows_wide
        * lax.rsqrt(jnp.mean(rows_wide * rows_wide, axis=-1, keepdims=True) + epsilon)
        * expert_norm_scale
    ).astype(BF16)
    taken, weight = routes(routed_expert_index.T, routed_expert_weight.T, experts, capacity)
    one_hot = taken.astype(BF16).reshape(experts * capacity, rows_local)
    mine = lax.dynamic_slice_in_dim(normed, lax.axis_index("tp") * col_width, col_width, 1)
    my_columns = jnp.dot(one_hot, mine, preferred_element_type=F32).astype(BF16)
    my_columns = my_columns.reshape(experts, capacity, col_width)
    arrived = lax.all_to_all(my_columns, "ep", split_axis=0, concat_axis=1, tiled=True)
    column_piece = lax.all_gather(arrived, "tp", axis=2, tiled=True)
    gate_pre = jnp.einsum(
        "esd,edf->esf", column_piece, routed_gate_weight, preferred_element_type=F32
    )
    up_pre = jnp.einsum("esd,edf->esf", column_piece, routed_up_weight, preferred_element_type=F32)
    hidden = (jax.nn.silu(gate_pre) * up_pre).astype(BF16)
    shared_hidden = (
        jax.nn.silu(jnp.dot(normed, shared_gate_weight, preferred_element_type=F32))
        * jnp.dot(normed, shared_up_weight, preferred_element_type=F32)
    ).astype(BF16)
    whole_mix, whole_hidden, whole_shared = one_gather(
        (mixer_normed, hidden, shared_hidden), "tp", (1, 2, 1)
    )
    mixer_output = jnp.dot(whole_mix, mixer_output_weight, preferred_element_type=F32).astype(BF16)
    expert_result = jnp.einsum(
        "esf,efd->esd", whole_hidden, routed_down_weight, preferred_element_type=F32
    ).astype(BF16)
    returned = lax.all_to_all(expert_result, "ep", split_axis=1, concat_axis=0, tiled=True)
    returned = returned.reshape(experts * capacity, col_width)
    weight_high = high(weight)
    contract = (((0,), (0,)), ((), ()))
    routed_sum = jnp.zeros((rows_local, col_width), F32)
    for part in (weight_high, weight - weight_high):
        spread_part = jnp.where(taken, part[:, None, :], 0.0).astype(BF16)
        spread_part = spread_part.reshape(experts * capacity, rows_local)
        routed_sum = routed_sum + lax.dot_general(
            spread_part, returned, contract, preferred_element_type=F32
        )
    shared_result = jnp.dot(whole_shared, shared_down_weight, preferred_element_type=F32)
    routed_out = (routed_sum + shared_result).astype(BF16)
    return (mixer_output, routed_out)


def solution(mesh):
    return jax.shard_map(
        on_device,
        mesh=mesh,
        in_specs=(
            P("ep", "tp"),
            P("ep", "tp"),
            P("ep", "tp"),
            P("ep", "tp"),
            P("ep", "tp"),
            P("ep", "tp"),
            P("tp"),
            P("tp"),
            P(None, "tp"),
            P(None, "tp"),
            P(None, "tp"),
            P("tp"),
            P(None, "tp"),
            P("ep", None),
            P(),
            P("ep", None),
            P("ep", None),
            P("ep", None, "tp"),
            P("ep", None, "tp"),
            P("ep", None, "tp"),
            P(None, "tp"),
            P(None, "tp"),
            P(None, "tp"),
        ),
        out_specs=(P("ep", "tp"), P("ep", "tp")),
        check_vma=False,
    )
```

profile of v0, /device:TPU:1, one launch (start us, length us, event | category | flops | bytes accessed | tf_op | source)
XLA Modules:
  0.0 346.0 jit_solution(6306174903025940382)
XLA Ops:
  9.6 4.9 %collective-permute-start = (bf16[3,512]{0,1:T(8,128)(2,1)S(1)}, bf16[3,512]{0,1:T(8,128)(2,1)S(1)}, u32[]{:S(2)}, u32[]{:S(2)}) collective-permute-start(bf16[3,512]{0,1:T(8,128)(2,1)S(1)} %copy.162), channel_id=1, source_target_pairs={{0,16},{16,32},{32,48},{48,64},{64,80},{80,96},{96,112},{112,128},... | collective-permute-start | bytes 9224 | tf_op jit(solution)/shard_map/ppermute | solution.py:19
  26.0 44.8 %all_to_all.33 = bf16[64,24,128]{2,1,0:T(8,128)(2,1)S(1)} all-to-all(bf16[64,24,128]{2,1,0:T(8,128)(2,1)S(1)} %bitcast.139), channel_id=1, replica_groups=mesh['ep'=32,'tp'=16] {'ep'}, dimensions={0} | all-to-all | bytes 786432 | tf_op jit(solution)/shard_map/all_to_all | solution.py:202
  72.1 1.4 fusion.74
  73.6 1.4 fusion.9
  75.7 28.7 %all-gather.5.cloned.1.call-done = bf16[32,272,128]{2,1,0:T(8,128)(2,1)} async-done(((bf16[1,272,128]{2,1,0:T(8,128)(2,1)}), bf16[32,272,128]{2,1,0:T(8,128)(2,1)}) %all-gather.5.cloned.1.call-update) | async-done | bytes 2228240 | tf_op jit(solution)/shard_map/all_gather | solution.py:67
  105.8 3.3 multiply_reduce_fusion
  110.6 73.3 %all-gather.7.cloned.1.call-done = bf16[2,768,2048]{2,1,0:T(8,128)(2,1)} async-done(((bf16[2,768,128]{2,1,0:T(8,128)(2,1)}), bf16[2,768,2048]{2,1,0:T(8,128)(2,1)}) %all-gather.7.cloned.1.call-update) | async-done | bytes 6291472 | tf_op jit(solution)/shard_map/all_gather | solution.py:203
  183.9 5.0 %fusion.73 = f32[2,768,64]{1,2,0:T(8,128)S(1)} fusion(bf16[2,768,2048]{2,1,0:T(8,128)(2,1)} %all-gather.7.cloned.1.call-done, bf16[2,2048,64]{1,2,0:T(8,128)(2,1)S(1)} %copy-done.8), kind=kOutput, calls=%fused_computation.151 | convolution fusion | flops 402653184 | bytes 7208960 | tf_op jit(solution)/shard_map/esd,edf->esf/dot_general | solution.py:204
  188.9 2.0 fusion.5
  192.1 74.8 %all-gather.9.cloned.1.call-done = bf16[2883584]{0:T(1024)(128)(2,1)} async-done(((bf16[180224]{0:T(1024)(128)(2,1)}), bf16[2883584]{0:T(1024)(128)(2,1)}) %all-gather.9.cloned.1.call-update) | async-done | bytes 5767184 | tf_op jit(solution)/shard_map/all_gather | solution.py:40
  266.9 5.8 %reshape.648 = bf16[16,180224]{1,0:T(8,128)(2,1)} reshape(bf16[2883584]{0:T(1024)(128)(2,1)} %all-gather.9.cloned.1.call-done) | data formatting | bytes 11534336 | tf_op jit(solution)/shard_map/all_gather | solution.py:40
  272.7 3.7 %slice.215 = bf16[16,98304]{1,0:T(8,128)(2,1)} slice(bf16[16,180224]{1,0:T(8,128)(2,1)} %reshape.648), slice={[0:16], [65536:163840]} | slice | bytes 6291456 | tf_op jit(solution)/shard_map/slice | solution.py:42
  276.4 8.8 %reshape.642 = bf16[16,2,768,64]{3,2,1,0:T(8,128)(2,1)} reshape(bf16[16,98304]{1,0:T(8,128)(2,1)} %slice.215) | data formatting | bytes 6291456 | tf_op jit(solution)/shard_map/reshape | solution.py:42
  285.3 6.9 %copy.183 = bf16[2,768,16,64]{1,3,2,0:T(8,128)(2,1)} copy(bf16[2,768,16,64]{3,1,0,2:T(8,128)(2,1)} %bitcast.127) | data formatting | bytes 6291456 | tf_op jit(solution)/shard_map/transpose | solution.py:33
  292.2 3.3 convolution_convert_fusion.1
  295.5 1.2 copy.185
  296.6 13.2 %all-to-all-start.1 = ((bf16[2,768,128]{2,0,1:T(2,128)(2,1)}), bf16[2,768,128]{2,0,1:T(2,128)(2,1)S(1)}, u32[]{:S(2)}, u32[]{:S(2)}) async-start(bf16[2,768,128]{2,0,1:T(2,128)(2,1)} %copy.185), calls=%async_computation.1 | async-start | bytes 786432 | tf_op jit(solution)/shard_map/all_to_all | solution.py:220
  309.9 1.8 fusion.4
  311.7 3.1 slice.210
  316.0 1.1 copy.188
  317.1 2.0 copy.194
  319.2 2.4 copy.182
  321.6 3.0 convolution_convert_fusion.2
  324.6 12.9 %all-to-all-done.1 = bf16[2,768,128]{2,0,1:T(2,128)(2,1)S(1)} async-done(((bf16[2,768,128]{2,0,1:T(2,128)(2,1)}), bf16[2,768,128]{2,0,1:T(2,128)(2,1)S(1)}, u32[]{:S(2)}, u32[]{:S(2)}) %all-to-all-start.1) | async-done | bytes 393248 | tf_op jit(solution)/shard_map/all_to_all | solution.py:220
  (170 shorter events, 22.6 us)
Async XLA Ops:
  7.2 314.4 %copy-start = (bf16[4096,128]{1,0:T(8,128)(2,1)S(1)}, bf16[4096,128]{1,0:T(8,128)(2,1)}, u32[]{:S(2)}) copy-start(bf16[4096,128]{1,0:T(8,128)(2,1)} %param.35) | copy-start | bytes 3145732
  7.2 15.1 %copy-start.18 = (bf16[256,128]{1,0:T(8,128)(2,1)S(1)}, bf16[256,128]{1,0:T(8,128)(2,1)}, u32[]{:S(2)}) copy-start(bf16[256,128]{1,0:T(8,128)(2,1)} %param.24) | copy-start | bytes 196612
  7.2 97.2 %all-gather.5.cloned.1.call-start = ((), (), s32[]{:S(2)}) async-start(), calls=%async_computation.2 | async-start | bytes 2297856 | tf_op jit(solution)/shard_map/all_gather | solution.py:67
  9.6 10.7 %collective-permute-start = (bf16[3,512]{0,1:T(8,128)(2,1)S(1)}, bf16[3,512]{0,1:T(8,128)(2,1)S(1)}, u32[]{:S(2)}, u32[]{:S(2)}) collective-permute-start(bf16[3,512]{0,1:T(8,128)(2,1)S(1)} %copy.162), channel_id=1, source_target_pairs={{0,16},{16,32},{32,48},{48,64},{64,80},{80,96},{96,112},{112,128},... | collective-permute-start | bytes 9224 | tf_op jit(solution)/shard_map/ppermute | solution.py:19
  24.2 159.7 %all-gather.7.cloned.1.call-start = ((), (), s32[]{:S(2)}) async-start(), calls=%async_computation.3 | async-start | bytes 6684672 | tf_op jit(solution)/shard_map/all_gather | solution.py:203
  25.5 46.2 %copy-start.33 = (f32[4]{0:T(128)S(1)}, f32[4]{0:T(128)}, u32[]{:S(2)}) copy-start(f32[4]{0:T(128)} %param.30) | copy-start | bytes 52
  25.6 46.4 %copy-start.15 = (bf16[256,256]{1,0:T(8,128)(2,1)S(1)}, bf16[256,256]{1,0:T(8,128)(2,1)}, u32[]{:S(2)}) copy-start(bf16[256,256]{1,0:T(8,128)(2,1)} %param.26) | copy-start | bytes 393220
  25.6 46.5 %copy-start.9 = (f32[2,128,4]{2,1,0:T(8,128)S(1)}, f32[2,128,4]{2,1,0:T(8,128)}, u32[]{:S(2)}) copy-start(f32[2,128,4]{2,1,0:T(8,128)} %get-tuple-element.13) | copy-start | bytes 12292
  71.6 195.3 %all-gather.9.cloned.1.call-start = ((), (), s32[]{:S(2)}) async-start(), calls=%async_computation.4 | async-start | bytes 6127616 | tf_op jit(solution)/shard_map/all_gather | solution.py:40
  73.5 35.6 %copy-start.10 = (f32[1,4,64,128]{3,2,1,0:T(8,128)S(1)}, f32[1,4,64,128]{3,2,1,0:T(8,128)}, u32[]{:S(2)}) copy-start(f32[1,4,64,128]{3,2,1,0:T(8,128)} %get-tuple-element.7) | copy-start | bytes 393220
  75.0 34.5 %copy-start.17 = (bf16[2,128,4,64]{1,0,3,2:T(2,128)(2,1)S(1)}, bf16[2,128,4,64]{1,0,3,2:T(2,128)(2,1)}, u32[]{:S(2)}) copy-start(bf16[2,128,4,64]{1,0,3,2:T(2,128)(2,1)} %get-tuple-element.5) | copy-start | bytes 393220
  109.1 74.8 %copy-start.8 = (bf16[2,2048,64]{1,2,0:T(8,128)(2,1)S(1)}, bf16[2,2048,64]{1,2,0:T(8,128)(2,1)}, u32[]{:S(2)}) copy-start(bf16[2,2048,64]{1,2,0:T(8,128)(2,1)} %param.40) | copy-start | bytes 1572868
  110.6 78.3 %copy-start.34 = (bf16[2,2048,64]{1,2,0:T(8,128)(2,1)S(1)}, bf16[2,2048,64]{1,2,0:T(8,128)(2,1)}, u32[]{:S(2)}) copy-start(bf16[2,2048,64]{1,2,0:T(8,128)(2,1)} %param.41) | copy-start | bytes 1572868
  285.3 6.9 %copy-start.11 = (bf16[2,1024,128]{2,1,0:T(8,128)(2,1)S(1)}, bf16[2,1024,128]{2,1,0:T(8,128)(2,1)}, u32[]{:S(2)}) copy-start(bf16[2,1024,128]{2,1,0:T(8,128)(2,1)} %param.42) | copy-start | bytes 1572868
  292.2 17.7 %copy-start.28 = (f32[256,4]{0,1:T(4,128)S(1)}, f32[256,4]{0,1:T(4,128)}, u32[]{:S(2)}) copy-start(f32[256,4]{0,1:T(4,128)} %param.39) | copy-start | bytes 12292
  292.2 17.7 %copy-start.22 = (s32[1,256]{1,0:T(1,128)S(1)}, s32[1,256]{1,0:T(1,128)}, u32[]{:S(2)}) copy-start(s32[1,256]{1,0:T(1,128)} %copy-done.21) | copy-start | bytes 3076
  292.2 17.7 %copy-start.24 = (s32[1,256]{1,0:T(1,128)S(1)}, s32[1,256]{1,0:T(1,128)}, u32[]{:S(2)}) copy-start(s32[1,256]{1,0:T(1,128)} %copy-done.23) | copy-start | bytes 3076
  292.2 17.7 %copy-start.26 = (s32[1,256]{1,0:T(1,128)S(1)}, s32[1,256]{1,0:T(1,128)}, u32[]{:S(2)}) copy-start(s32[1,256]{1,0:T(1,128)} %copy-done.25) | copy-start | bytes 3076
  292.2 17.7 %copy-start.13 = (f32[64,256]{1,0:T(8,128)S(1)}, f32[64,256]{1,0:T(8,128)}, u32[]{:S(2)}) copy-start(f32[64,256]{1,0:T(8,128)} %copy-done.12) | copy-start | bytes 196612
  292.2 17.7 %copy-start.30 = (f32[24]{0:T(128)S(1)}, f32[24]{0:T(128)}, u32[]{:S(2)}) copy-start(f32[24]{0:T(128)} %copy-done.29) | copy-start | bytes 292
  296.6 40.9 %all-to-all-start.1 = ((bf16[2,768,128]{2,0,1:T(2,128)(2,1)}), bf16[2,768,128]{2,0,1:T(2,128)(2,1)S(1)}, u32[]{:S(2)}, u32[]{:S(2)}) async-start(bf16[2,768,128]{2,0,1:T(2,128)(2,1)} %copy.185), calls=%async_computation.1 | async-start | bytes 786432 | tf_op jit(solution)/shard_map/all_to_all | solution.py:220
  321.6 16.1 %copy-start.3 = (bf16[64,24,256]{2,1,0:T(8,128)(2,1)S(1)}, bf16[64,24,256]{2,1,0:T(8,128)(2,1)}, u32[]{:S(2)}) copy-start(bf16[64,24,256]{2,1,0:T(8,128)(2,1)} %get-tuple-element.18) | copy-start | bytes 2359300
  324.6 13.4 %copy-start.4 = (bf16[64,24,256]{2,1,0:T(8,128)(2,1)S(1)}, bf16[64,24,256]{2,1,0:T(8,128)(2,1)}, u32[]{:S(2)}) copy-start(bf16[64,24,256]{2,1,0:T(8,128)(2,1)} %get-tuple-element.17) | copy-start | bytes 2359300
  324.6 13.9 %copy-start.5 = (bf16[256,16,64]{0,2,1:T(8,128)(2,1)S(1)}, bf16[256,16,64]{0,2,1:T(8,128)(2,1)}, u32[]{:S(2)}) copy-start(bf16[256,16,64]{0,2,1:T(8,128)(2,1)} %copy.188) | copy-start | bytes 1572868
  (17 other events, 49.9 us)
Sparse Core Ops, SparseCore 0:
  24.3 80.0 all-gather.4
  107.4 76.4 all-gather.6
  192.2 74.6 all-gather.8
where the time goes:
time: 347 us; the launch traced here: 346 us
  waiting for transfers between devices  190 us (55%)
  local copies, waits for them, and re-layouts  46.7 us (13%)
  blocking collectives  44.8 us (13%)
  matrix products  19.5 us (6%)
  starting transfers between devices  18.2 us (5%)
  between operations  14.5 us (4%)
  other arithmetic  12.5 us (4%)
    all_gather x1, waiting for transfers between devices, one_gather(): lines, at, finished = (lax.all_gather(ravelled, axis), 0, [])  74.8 us
    all_gather x1, waiting for transfers between devices, on_device(): column_piece = lax.all_gather(arrived, 'tp', axis=2, tiled=True)  73.3 us
    all_to_all x1, blocking collectives, on_device(): lax.all_to_all(my_columns, 'ep', split_axis=0, concat_axis=1, tiled=True)  44.8 us
    all_gather x1, waiting for transfers between devices, state_before(): gathered = lax.all_gather(payload, 'ep')  28.7 us
    all_to_all x1, starting transfers between devices, on_device(): lax.all_to_all(expert_result, 'ep', split_axis=1, concat_axis=0, tiled=True)  13.2 us
    all_to_all x1, waiting for transfers between devices, on_device(): lax.all_to_all(expert_result, 'ep', split_axis=1, concat_axis=0, tiled=True)  12.9 us
    transpose x3, local copies, waits for them, and re-layouts, laid_out(): tiles = jnp.moveaxis(tiles, 0, dim)  10.4 us
    reshape x2, local copies, waits for them, and re-layouts, one_gather(): tiles = lines[:, at:at + a.size].reshape(-1, *a.shape)  9.96 us
  transfers between devices with their start and end apart: 5, of which 4 were waited for; matrix products, arithmetic and copies ran while one was open for 9% of the time, Pallas kernels for 0%

commit v1 on v0

--- a/solution.py
+++ b/solution.py
@@ -200,7 +200,16 @@
     my_columns = jnp.dot(one_hot, mine, preferred_element_type=F32).astype(BF16)
     my_columns = my_columns.reshape(experts, capacity, col_width)
     arrived = lax.all_to_all(my_columns, "ep", split_axis=0, concat_axis=1, tiled=True)
-    column_piece = lax.all_gather(arrived, "tp", axis=2, tiled=True)
+    ways = lax.axis_size("tp")
+    up = [(d, (d + 1) % ways) for d in range(ways)]
+    down = [(d, (d - 1) % ways) for d in range(ways)]
+    earlier_2, later = ([arrived], [arrived])
+    for _ in range(ways // 2):
+        earlier_2.append(lax.ppermute(earlier_2[-1], "tp", up))
+    for _ in range((ways - 1) // 2):
+        later.append(lax.ppermute(later[-1], "tp", down))
+    line = jnp.concatenate([*earlier_2[::-1], *later[1:]], axis=2)
+    column_piece = jnp.roll(line, (lax.axis_index("tp") - ways // 2) * arrived.shape[2], axis=2)
     gate_pre = jnp.einsum(
         "esd,edf->esf", column_piece, routed_gate_weight, preferred_element_type=F32
     )

time: 347 us -> 362 us (1.043)
  starting transfers between devices: 18.2 us -> 97.3 us
  waiting for transfers between devices: 190 us -> 119 us
  blocking collectives: 44.8 us -> 0 us
  local copies, waits for them, and re-layouts: 46.7 us -> 84 us
  other arithmetic: 12.5 us -> 21.2 us
    all_gather x1 -> x0, waiting for transfers between devices: 73.3 us -> none  [on_device(): column_piece = lax.all_gather(arrived, 'tp', axis=2, tiled=True)]
    ppermute x0 -> x15, starting transfers between devices: none -> 63.8 us  [the longest x7 47.1 us: on_device(): later.append(lax.ppermute(later[-1], 'tp', down))]
    all_to_all x1 -> x0, blocking collectives: 44.8 us -> none  [on_device(): lax.all_to_all(my_columns, 'ep', split_axis=0, concat_axis=1, tiled=True)]
    all_gather x1, waiting for transfers between devices: 28.7 us -> 0.02 us  [state_before(): gathered = lax.all_gather(payload, 'ep')]
    unnamed x75 -> x60, local copies, waits for them, and re-layouts: 3.53 us -> 30.4 us
    ppermute x0 -> x15, waiting for transfers between devices: none -> 20.9 us  [the longest x8 18 us: on_device(): earlier_2.append(lax.ppermute(earlier_2[-1], 'tp', up))]
    all_to_all x0 -> x1, starting transfers between devices: none -> 16.7 us  [on_device(): lax.all_to_all(my_columns, 'ep', split_axis=0, concat_axis=1, tiled=True)]
    ppermute x1, waiting for transfers between devices: 0.01 us -> 5.74 us  [passed_along(): return lax.ppermute(x, axis, pairs)]
  transfers between devices with their start and end apart: 5 -> 20, of which waited for: 4 -> 12; matrix products, arithmetic and copies ran while one was open for 9% -> 19% of each run, Pallas kernels for 0% -> 0%
where the time goes in v1:
time: 362 us; the launch traced here: 359 us
  waiting for transfers between devices  119 us (33%)
  starting transfers between devices  97.3 us (27%)
  local copies, waits for them, and re-layouts  84 us (23%)
  matrix products  23.1 us (6%)
  other arithmetic  21.2 us (6%)
  between operations  14.9 us (4%)
    all_gather x1, waiting for transfers between devices, one_gather(): lines, at, finished = (lax.all_gather(ravelled, axis), 0, [])  75.9 us
    ppermute x7, starting transfers between devices, on_device(): later.append(lax.ppermute(later[-1], 'tp', down))  47.1 us
    unnamed x60, local copies, waits for them, and re-layouts  30.4 us
    ppermute x8, waiting for transfers between devices, on_device(): earlier_2.append(lax.ppermute(earlier_2[-1], 'tp', up))  18 us
    all_to_all x1, starting transfers between devices, on_device(): lax.all_to_all(my_columns, 'ep', split_axis=0, concat_axis=1, tiled=True)  16.7 us
    ppermute x8, starting transfers between devices, on_device(): earlier_2.append(lax.ppermute(earlier_2[-1], 'tp', up))  16.7 us
    all_to_all x1, starting transfers between devices, on_device(): lax.all_to_all(expert_result, 'ep', split_axis=1, concat_axis=0, tiled=True)  13.2 us
    transpose x3, local copies, waits for them, and re-layouts, laid_out(): tiles = jnp.moveaxis(tiles, 0, dim)  12.2 us
  transfers between devices with their start and end apart: 20, of which 12 were waited for; matrix products, arithmetic and copies ran while one was open for 19% of the time, Pallas kernels for 0%

profile of v1, /device:TPU:1, one launch (start us, length us, event | category | flops | bytes accessed | tf_op | source)
XLA Modules:
  0.0 359.4 jit_solution(10096136277656162502)
XLA Ops:
  13.6 16.7 %all-to-all-start = ((bf16[64,24,128]{2,1,0:T(8,128)(2,1)}), bf16[64,24,128]{2,1,0:T(8,128)(2,1)S(1)}, u32[]{:S(2)}, u32[]{:S(2)}) async-start(bf16[64,24,128]{2,1,0:T(8,128)(2,1)} %bitcast.34), calls=%async_computation | async-start | bytes 786432 | tf_op jit(solution)/shard_map/all_to_all | solution.py:202
  32.7 3.5 collective-permute-start
  41.9 5.7 %collective-permute-done = bf16[3,512]{0,1:T(8,128)(2,1)S(1)} collective-permute-done((bf16[3,512]{0,1:T(8,128)(2,1)S(1)}, bf16[3,512]{0,1:T(8,128)(2,1)S(1)}, u32[]{:S(2)}, u32[]{:S(2)}) %collective-permute-start) | collective-permute-done | bytes 3104 | tf_op jit(solution)/shard_map/ppermute | solution.py:19
  52.6 5.4 %all-to-all-done = bf16[64,24,128]{2,1,0:T(8,128)(2,1)S(1)} async-done(((bf16[64,24,128]{2,1,0:T(8,128)(2,1)}), bf16[64,24,128]{2,1,0:T(8,128)(2,1)S(1)}, u32[]{:S(2)}, u32[]{:S(2)}) %all-to-all-start) | async-done | bytes 393248 | tf_op jit(solution)/shard_map/all_to_all | solution.py:202
  58.1 3.1 collective-permute-start.1
  61.2 5.6 %collective-permute-start.9 = (bf16[2,768,128]{2,1,0:T(8,128)(2,1)S(1)}, bf16[2,768,128]{2,1,0:T(8,128)(2,1)S(1)}, u32[]{:S(2)}, u32[]{:S(2)}) collective-permute-start(bf16[2,768,128]{2,1,0:T(8,128)(2,1)S(1)} %bitcast.132), channel_id=1, source_target_pairs={{0,15},{1,0},{2,1},{3,2},{4,3},{5,4},{6,5},{7,6},{8,7},{9,8},{10,9... | collective-permute-start | bytes 1179656 | tf_op jit(solution)/shard_map/ppermute | solution.py:210
  66.9 6.4 %collective-permute-done.1 = bf16[2,768,128]{2,1,0:T(8,128)(2,1)S(1)} collective-permute-done((bf16[2,768,128]{2,1,0:T(8,128)(2,1)S(1)}, bf16[2,768,128]{2,1,0:T(8,128)(2,1)S(1)}, u32[]{:S(2)}, u32[]{:S(2)}) %collective-permute-start.1) | collective-permute-done | bytes 393248 | tf_op jit(solution)/shard_map/ppermute | solution.py:208
  75.2 6.7 %collective-permute-start.10 = (bf16[2,768,128]{2,1,0:T(8,128)(2,1)S(1)}, bf16[2,768,128]{2,1,0:T(8,128)(2,1)}, u32[]{:S(2)}, u32[]{:S(2)}) collective-permute-start(bf16[2,768,128]{2,1,0:T(8,128)(2,1)S(1)} %collective-permute-done.9), channel_id=1, source_target_pairs={{0,15},{1,0},{2,1},{3,2},{4,3},{5,4},{6,5},{7,6},{8,7},{9,8},{10,9... | collective-permute-start | bytes 1179656 | tf_op jit(solution)/shard_map/ppermute | solution.py:210
  81.9 5.7 %collective-permute-done.2 = bf16[2,768,128]{2,1,0:T(8,128)(2,1)} collective-permute-done((bf16[2,768,128]{2,1,0:T(8,128)(2,1)S(1)}, bf16[2,768,128]{2,1,0:T(8,128)(2,1)}, u32[]{:S(2)}, u32[]{:S(2)}) %collective-permute-start.2) | collective-permute-done | bytes 393248 | tf_op jit(solution)/shard_map/ppermute | solution.py:208
  90.2 6.7 %collective-permute-start.11 = (bf16[2,768,128]{2,1,0:T(8,128)(2,1)}, bf16[2,768,128]{2,1,0:T(8,128)(2,1)}, u32[]{:S(2)}, u32[]{:S(2)}) collective-permute-start(bf16[2,768,128]{2,1,0:T(8,128)(2,1)} %collective-permute-done.10), channel_id=1, source_target_pairs={{0,15},{1,0},{2,1},{3,2},{4,3},{5,4},{6,5},{7,6},{8,7},{9,8},{10,9... | collective-permute-start | bytes 1179656 | tf_op jit(solution)/shard_map/ppermute | solution.py:210
  96.8 4.4 %collective-permute-done.3 = bf16[2,768,128]{2,1,0:T(8,128)(2,1)} collective-permute-done((bf16[2,768,128]{2,1,0:T(8,128)(2,1)}, bf16[2,768,128]{2,1,0:T(8,128)(2,1)}, u32[]{:S(2)}, u32[]{:S(2)}) %collective-permute-start.3) | collective-permute-done | bytes 393248 | tf_op jit(solution)/shard_map/ppermute | solution.py:208
  113.2 6.7 %collective-permute-start.12 = (bf16[2,768,128]{2,1,0:T(8,128)(2,1)}, bf16[2,768,128]{2,1,0:T(8,128)(2,1)S(1)}, u32[]{:S(2)}, u32[]{:S(2)}) collective-permute-start(bf16[2,768,128]{2,1,0:T(8,128)(2,1)} %collective-permute-done.11), channel_id=1, source_target_pairs={{0,15},{1,0},{2,1},{3,2},{4,3},{5,4},{6,5},{7,6},{8,7},{9,8},{10,9... | collective-permute-start | bytes 1179656 | tf_op jit(solution)/shard_map/ppermute | solution.py:210
  124.9 7.4 %collective-permute-start.13 = (bf16[2,768,128]{2,1,0:T(8,128)(2,1)S(1)}, bf16[2,768,128]{2,1,0:T(8,128)(2,1)S(1)}, u32[]{:S(2)}, u32[]{:S(2)}) collective-permute-start(bf16[2,768,128]{2,1,0:T(8,128)(2,1)S(1)} %collective-permute-done.12), channel_id=1, source_target_pairs={{0,15},{1,0},{2,1},{3,2},{4,3},{5,4},{6,5},{7,6},{8,7},{9,8},{10,9... | collective-permute-start | bytes 1179656 | tf_op jit(solution)/shard_map/ppermute | solution.py:210
  137.0 7.1 %collective-permute-start.14 = (bf16[2,768,128]{2,1,0:T(8,128)(2,1)S(1)}, bf16[2,768,128]{2,1,0:T(8,128)(2,1)}, u32[]{:S(2)}, u32[]{:S(2)}) collective-permute-start(bf16[2,768,128]{2,1,0:T(8,128)(2,1)S(1)} %collective-permute-done.13), channel_id=1, source_target_pairs={{0,15},{1,0},{2,1},{3,2},{4,3},{5,4},{6,5},{7,6},{8,7},{9,8},{10,9... | collective-permute-start | bytes 1179656 | tf_op jit(solution)/shard_map/ppermute | solution.py:210
  149.2 6.9 %collective-permute-start.15 = (bf16[2,768,128]{2,1,0:T(8,128)(2,1)}, bf16[2,768,128]{2,1,0:T(8,128)(2,1)}, u32[]{:S(2)}, u32[]{:S(2)}) collective-permute-start(bf16[2,768,128]{2,1,0:T(8,128)(2,1)} %collective-permute-done.14), channel_id=1, source_target_pairs={{0,15},{1,0},{2,1},{3,2},{4,3},{5,4},{6,5},{7,6},{8,7},{9,8},{10,9... | collective-permute-start | bytes 1179656 | tf_op jit(solution)/shard_map/ppermute | solution.py:210
  160.1 3.2 multiply_reduce_fusion
  200.5 75.9 %all-gather.6.cloned.1.call-done = bf16[2883584]{0:T(1024)(128)(2,1)} async-done(((bf16[180224]{0:T(1024)(128)(2,1)}), bf16[2883584]{0:T(1024)(128)(2,1)}) %all-gather.6.cloned.1.call-update) | async-done | bytes 5767184 | tf_op jit(solution)/shard_map/all_gather | solution.py:40
  276.4 5.8 %reshape.648 = bf16[16,180224]{1,0:T(8,128)(2,1)} reshape(bf16[2883584]{0:T(1024)(128)(2,1)} %all-gather.6.cloned.1.call-done) | data formatting | bytes 11534336 | tf_op jit(solution)/shard_map/all_gather | solution.py:40
  282.2 3.8 %slice.215 = bf16[16,98304]{1,0:T(8,128)(2,1)} slice(bf16[16,180224]{1,0:T(8,128)(2,1)} %reshape.648), slice={[0:16], [65536:163840]} | slice | bytes 6291456 | tf_op jit(solution)/shard_map/slice | solution.py:42
  286.0 8.8 %reshape.642 = bf16[16,2,768,64]{3,2,1,0:T(8,128)(2,1)} reshape(bf16[16,98304]{1,0:T(8,128)(2,1)} %slice.215) | data formatting | bytes 6291456 | tf_op jit(solution)/shard_map/reshape | solution.py:42
  294.8 7.0 %copy.183 = bf16[2,768,16,64]{1,3,2,0:T(8,128)(2,1)} copy(bf16[2,768,16,64]{3,1,0,2:T(8,128)(2,1)} %bitcast.125) | data formatting | bytes 6291456 | tf_op jit(solution)/shard_map/transpose | solution.py:33
  301.8 3.3 convolution_convert_fusion.1
  306.3 13.2 %all-to-all-start.1 = ((bf16[2,768,128]{2,0,1:T(2,128)(2,1)}), bf16[2,768,128]{2,0,1:T(2,128)(2,1)S(1)}, u32[]{:S(2)}, u32[]{:S(2)}) async-start(bf16[2,768,128]{2,0,1:T(2,128)(2,1)} %copy.185), calls=%async_computation.1 | async-start | bytes 786432 | tf_op jit(solution)/shard_map/all_to_all | solution.py:229
  336.3 11.0 %all-to-all-done.1 = bf16[2,768,128]{2,0,1:T(2,128)(2,1)S(1)} async-done(((bf16[2,768,128]{2,0,1:T(2,128)(2,1)}), bf16[2,768,128]{2,0,1:T(2,128)(2,1)S(1)}, u32[]{:S(2)}, u32[]{:S(2)}) %all-to-all-start.1) | async-done | bytes 393248 | tf_op jit(solution)/shard_map/all_to_all | solution.py:229
  (184 shorter events, 114.4 us)
Async XLA Ops:
  7.2 327.7 %copy-start = (bf16[4096,128]{1,0:T(8,128)(2,1)S(1)}, bf16[4096,128]{1,0:T(8,128)(2,1)}, u32[]{:S(2)}) copy-start(bf16[4096,128]{1,0:T(8,128)(2,1)} %param.35) | copy-start | bytes 3145732
  13.6 44.5 %all-to-all-start = ((bf16[64,24,128]{2,1,0:T(8,128)(2,1)}), bf16[64,24,128]{2,1,0:T(8,128)(2,1)S(1)}, u32[]{:S(2)}, u32[]{:S(2)}) async-start(bf16[64,24,128]{2,1,0:T(8,128)(2,1)} %bitcast.34), calls=%async_computation | async-start | bytes 786432 | tf_op jit(solution)/shard_map/all_to_all | solution.py:202
  30.3 128.4 %all-gather.4.cloned.1.call-start = ((), (), s32[]{:S(2)}) async-start(), calls=%async_computation.2 | async-start | bytes 2297856 | tf_op jit(solution)/shard_map/all_gather | solution.py:67
  32.7 15.0 %collective-permute-start = (bf16[3,512]{0,1:T(8,128)(2,1)S(1)}, bf16[3,512]{0,1:T(8,128)(2,1)S(1)}, u32[]{:S(2)}, u32[]{:S(2)}) collective-permute-start(bf16[3,512]{0,1:T(8,128)(2,1)S(1)} %copy.162), channel_id=1, source_target_pairs={{0,16},{16,32},{32,48},{48,64},{64,80},{80,96},{96,112},{112,128},... | collective-permute-start | bytes 9224 | tf_op jit(solution)/shard_map/ppermute | solution.py:19
  52.6 223.8 %all-gather.6.cloned.1.call-start = ((), (), s32[]{:S(2)}) async-start(), calls=%async_computation.3 | async-start | bytes 6127616 | tf_op jit(solution)/shard_map/all_gather | solution.py:40
  58.1 15.2 %collective-permute-start.1 = (bf16[2,768,128]{2,1,0:T(8,128)(2,1)S(1)}, bf16[2,768,128]{2,1,0:T(8,128)(2,1)S(1)}, u32[]{:S(2)}, u32[]{:S(2)}) collective-permute-start(bf16[2,768,128]{2,1,0:T(8,128)(2,1)S(1)} %bitcast.131), channel_id=1, source_target_pairs={{0,1},{1,2},{2,3},{3,4},{4,5},{5,6},{6,7},{7,8},{8,9},{9,10},{10,1... | collective-permute-start | bytes 1179656 | tf_op jit(solution)/shard_map/ppermute | solution.py:208
  61.2 14.0 %collective-permute-start.9 = (bf16[2,768,128]{2,1,0:T(8,128)(2,1)S(1)}, bf16[2,768,128]{2,1,0:T(8,128)(2,1)S(1)}, u32[]{:S(2)}, u32[]{:S(2)}) collective-permute-start(bf16[2,768,128]{2,1,0:T(8,128)(2,1)S(1)} %bitcast.132), channel_id=1, source_target_pairs={{0,15},{1,0},{2,1},{3,2},{4,3},{5,4},{6,5},{7,6},{8,7},{9,8},{10,9... | collective-permute-start | bytes 1179656 | tf_op jit(solution)/shard_map/ppermute | solution.py:210
  73.3 14.3 %collective-permute-start.2 = (bf16[2,768,128]{2,1,0:T(8,128)(2,1)S(1)}, bf16[2,768,128]{2,1,0:T(8,128)(2,1)}, u32[]{:S(2)}, u32[]{:S(2)}) collective-permute-start(bf16[2,768,128]{2,1,0:T(8,128)(2,1)S(1)} %collective-permute-done.1), channel_id=1, source_target_pairs={{0,1},{1,2},{2,3},{3,4},{4,5},{5,6},{6,7},{7,8},{8,9},{9,10},{10,1... | collective-permute-start | bytes 1179656 | tf_op jit(solution)/shard_map/ppermute | solution.py:208
  75.2 14.9 %collective-permute-start.10 = (bf16[2,768,128]{2,1,0:T(8,128)(2,1)S(1)}, bf16[2,768,128]{2,1,0:T(8,128)(2,1)}, u32[]{:S(2)}, u32[]{:S(2)}) collective-permute-start(bf16[2,768,128]{2,1,0:T(8,128)(2,1)S(1)} %collective-permute-done.9), channel_id=1, source_target_pairs={{0,15},{1,0},{2,1},{3,2},{4,3},{5,4},{6,5},{7,6},{8,7},{9,8},{10,9... | collective-permute-start | bytes 1179656 | tf_op jit(solution)/shard_map/ppermute | solution.py:210
  87.6 13.6 %collective-permute-start.3 = (bf16[2,768,128]{2,1,0:T(8,128)(2,1)}, bf16[2,768,128]{2,1,0:T(8,128)(2,1)}, u32[]{:S(2)}, u32[]{:S(2)}) collective-permute-start(bf16[2,768,128]{2,1,0:T(8,128)(2,1)} %collective-permute-done.2), channel_id=1, source_target_pairs={{0,1},{1,2},{2,3},{3,4},{4,5},{5,6},{6,7},{7,8},{8,9},{9,10},{10,1... | collective-permute-start | bytes 1179656 | tf_op jit(solution)/shard_map/ppermute | solution.py:208
  90.2 23.0 %collective-permute-start.11 = (bf16[2,768,128]{2,1,0:T(8,128)(2,1)}, bf16[2,768,128]{2,1,0:T(8,128)(2,1)}, u32[]{:S(2)}, u32[]{:S(2)}) collective-permute-start(bf16[2,768,128]{2,1,0:T(8,128)(2,1)} %collective-permute-done.10), channel_id=1, source_target_pairs={{0,15},{1,0},{2,1},{3,2},{4,3},{5,4},{6,5},{7,6},{8,7},{9,8},{10,9... | collective-permute-start | bytes 1179656 | tf_op jit(solution)/shard_map/ppermute | solution.py:210
  101.3 18.6 %collective-permute-start.4 = (bf16[2,768,128]{2,1,0:T(8,128)(2,1)}, bf16[2,768,128]{2,1,0:T(8,128)(2,1)}, u32[]{:S(2)}, u32[]{:S(2)}) collective-permute-start(bf16[2,768,128]{2,1,0:T(8,128)(2,1)} %collective-permute-done.3), channel_id=1, source_target_pairs={{0,1},{1,2},{2,3},{3,4},{4,5},{5,6},{6,7},{7,8},{8,9},{9,10},{10,1... | collective-permute-start | bytes 1179656 | tf_op jit(solution)/shard_map/ppermute | solution.py:208
  113.2 11.7 %collective-permute-start.12 = (bf16[2,768,128]{2,1,0:T(8,128)(2,1)}, bf16[2,768,128]{2,1,0:T(8,128)(2,1)S(1)}, u32[]{:S(2)}, u32[]{:S(2)}) collective-permute-start(bf16[2,768,128]{2,1,0:T(8,128)(2,1)} %collective-permute-done.11), channel_id=1, source_target_pairs={{0,15},{1,0},{2,1},{3,2},{4,3},{5,4},{6,5},{7,6},{8,7},{9,8},{10,9... | collective-permute-start | bytes 1179656 | tf_op jit(solution)/shard_map/ppermute | solution.py:210
  119.9 12.4 %collective-permute-start.5 = (bf16[2,768,128]{2,1,0:T(8,128)(2,1)}, bf16[2,768,128]{2,1,0:T(8,128)(2,1)}, u32[]{:S(2)}, u32[]{:S(2)}) collective-permute-start(bf16[2,768,128]{2,1,0:T(8,128)(2,1)} %collective-permute-done.4), channel_id=1, source_target_pairs={{0,1},{1,2},{2,3},{3,4},{4,5},{5,6},{6,7},{7,8},{8,9},{9,10},{10,1... | collective-permute-start | bytes 1179656 | tf_op jit(solution)/shard_map/ppermute | solution.py:208
  124.9 12.1 %collective-permute-start.13 = (bf16[2,768,128]{2,1,0:T(8,128)(2,1)S(1)}, bf16[2,768,128]{2,1,0:T(8,128)(2,1)S(1)}, u32[]{:S(2)}, u32[]{:S(2)}) collective-permute-start(bf16[2,768,128]{2,1,0:T(8,128)(2,1)S(1)} %collective-permute-done.12), channel_id=1, source_target_pairs={{0,15},{1,0},{2,1},{3,2},{4,3},{5,4},{6,5},{7,6},{8,7},{9,8},{10,9... | collective-permute-start | bytes 1179656 | tf_op jit(solution)/shard_map/ppermute | solution.py:210
  132.3 12.2 %collective-permute-start.6 = (bf16[2,768,128]{2,1,0:T(8,128)(2,1)}, bf16[2,768,128]{2,1,0:T(8,128)(2,1)}, u32[]{:S(2)}, u32[]{:S(2)}) collective-permute-start(bf16[2,768,128]{2,1,0:T(8,128)(2,1)} %collective-permute-done.5), channel_id=1, source_target_pairs={{0,1},{1,2},{2,3},{3,4},{4,5},{5,6},{6,7},{7,8},{8,9},{9,10},{10,1... | collective-permute-start | bytes 1179656 | tf_op jit(solution)/shard_map/ppermute | solution.py:208
  137.0 12.2 %collective-permute-start.14 = (bf16[2,768,128]{2,1,0:T(8,128)(2,1)S(1)}, bf16[2,768,128]{2,1,0:T(8,128)(2,1)}, u32[]{:S(2)}, u32[]{:S(2)}) collective-permute-start(bf16[2,768,128]{2,1,0:T(8,128)(2,1)S(1)} %collective-permute-done.13), channel_id=1, source_target_pairs={{0,15},{1,0},{2,1},{3,2},{4,3},{5,4},{6,5},{7,6},{8,7},{9,8},{10,9... | collective-permute-start | bytes 1179656 | tf_op jit(solution)/shard_map/ppermute | solution.py:210
  144.5 12.1 %collective-permute-start.7 = (bf16[2,768,128]{2,1,0:T(8,128)(2,1)}, bf16[2,768,128]{2,1,0:T(8,128)(2,1)}, u32[]{:S(2)}, u32[]{:S(2)}) collective-permute-start(bf16[2,768,128]{2,1,0:T(8,128)(2,1)} %collective-permute-done.6), channel_id=1, source_target_pairs={{0,1},{1,2},{2,3},{3,4},{4,5},{5,6},{6,7},{7,8},{8,9},{9,10},{10,1... | collective-permute-start | bytes 1179656 | tf_op jit(solution)/shard_map/ppermute | solution.py:208
  149.2 31.7 %collective-permute-start.15 = (bf16[2,768,128]{2,1,0:T(8,128)(2,1)}, bf16[2,768,128]{2,1,0:T(8,128)(2,1)}, u32[]{:S(2)}, u32[]{:S(2)}) collective-permute-start(bf16[2,768,128]{2,1,0:T(8,128)(2,1)} %collective-permute-done.14), channel_id=1, source_target_pairs={{0,15},{1,0},{2,1},{3,2},{4,3},{5,4},{6,5},{7,6},{8,7},{9,8},{10,9... | collective-permute-start | bytes 1179656 | tf_op jit(solution)/shard_map/ppermute | solution.py:210
  156.6 12.1 %collective-permute-start.8 = (bf16[2,768,128]{2,1,0:T(8,128)(2,1)}, bf16[2,768,128]{2,1,0:T(8,128)(2,1)}, u32[]{:S(2)}, u32[]{:S(2)}) collective-permute-start(bf16[2,768,128]{2,1,0:T(8,128)(2,1)} %collective-permute-done.7), channel_id=1, source_target_pairs={{0,1},{1,2},{2,3},{3,4},{4,5},{5,6},{6,7},{7,8},{8,9},{9,10},{10,1... | collective-permute-start | bytes 1179656 | tf_op jit(solution)/shard_map/ppermute | solution.py:208
  286.0 34.4 %copy-start.8 = (s32[1,256]{1,0:T(1,128)S(1)}, s32[1,256]{1,0:T(1,128)}, u32[]{:S(2)}) copy-start(s32[1,256]{1,0:T(1,128)} %copy-done.7) | copy-start | bytes 3076
  286.0 34.4 %copy-start.10 = (s32[1,256]{1,0:T(1,128)S(1)}, s32[1,256]{1,0:T(1,128)}, u32[]{:S(2)}) copy-start(s32[1,256]{1,0:T(1,128)} %copy-done.9) | copy-start | bytes 3076
  294.8 30.0 %slice-start = ((bf16[16,180224]{1,0:T(8,128)(2,1)}), bf16[16,65536]{1,0:T(8,128)(2,1)S(1)}, s32[]{:S(2)}) async-start(bf16[16,180224]{1,0:T(8,128)(2,1)} %reshape.648), calls=%async_computation.4 | async-start | bytes 4194304 | tf_op jit(solution)/shard_map/slice | solution.py:42
  306.3 40.9 %all-to-all-start.1 = ((bf16[2,768,128]{2,0,1:T(2,128)(2,1)}), bf16[2,768,128]{2,0,1:T(2,128)(2,1)S(1)}, u32[]{:S(2)}, u32[]{:S(2)}) async-start(bf16[2,768,128]{2,0,1:T(2,128)(2,1)} %copy.185), calls=%async_computation.1 | async-start | bytes 786432 | tf_op jit(solution)/shard_map/all_to_all | solution.py:229
  (9 other events, 87.9 us)
Sparse Core Ops, SparseCore 0:
  52.7 75.2 all-gather.3
  200.6 75.7 all-gather.5
